TPU v7x, 512 devices: a whole 4x4x16 slice. The times are simulated.
512 devices in a mesh: sp: 16 (over z), dp: 32 (over y, x, core).
Axes of the slice: x: 4, y: 4, z: 16, core: 2. Of those that a mesh axis runs over, the one named last changes fastest.
Arguments:
- cotangent: bfloat16 [32, 2048, 2048], P('dp', 'sp'), may hold values from -6 to 6
- unit_pre: bfloat16 [32, 2048, 2048], P('dp', None, 'sp'), may hold values from -6 to 6
- gate_pre: bfloat16 [32, 2048, 2048], P('dp', None, 'sp'), may hold values from -15 to 15
- out_weight: bfloat16 [2048, 2048], P('dp', 'sp'), may hold values from -0.125 to 0.125
- mix_weight: bfloat16 [8, 128, 128], replicated, may hold values from -0.5 to 0.5
- mix_bias: bfloat16 [8, 128], replicated, may hold values from 0.099609375 to 1.8984375
- norm_gain: bfloat16 [2048], P('sp'), may hold values from 0.099609375 to 1.8984375
- norm_shift: bfloat16 [2048], P('sp'), may hold values from -3 to 3
Outputs:
- unit_grad: bfloat16 [32, 2048, 2048], P('dp', None, 'sp')
- gate_grad: bfloat16 [32, 2048, 2048], P('dp', None, 'sp')
- out_weight_grad: float32 [2048, 2048], P('dp', 'sp')
- mix_weight_grad: float32 [8, 128, 128], replicated
- mix_bias_grad: float32 [8, 128], replicated
- gain_grad: float32 [2048], P('sp')
- shift_grad: float32 [2048], P('sp')
All inputs are finite; a program needn't handle non-finite values.
Results may differ from a plain program's by a relative error of at most 0.015.
Values may be sent and summed in bfloat16 or wider, within the bound.
A program may use at most 64 MiB of HBM per device.

v0:
```python
import math
import jax
import jax.numpy as jnp
from jax import lax
from jax.sharding import PartitionSpec as P

GW = 2048
GROUPS = 8
BLK = 128
epsilon = 1e-05
tanh_coef = math.sqrt(2.0 / math.pi)


def sum_over(x, axis):
    devices = lax.axis_size(axis)
    copies = jnp.broadcast_to(x[None], (devices, *x.shape))
    return lax.all_to_all(copies, axis, 0, 0, tiled=True).sum(axis=0)


def gelu_slope(values):
    inner = tanh_coef * (values + 0.044715 * values * values * values)
    hyper = jnp.tanh(inner)
    return 0.5 * (1.0 + hyper) + 0.5 * values * (1.0 - hyper * hyper) * tanh_coef * (
        1.0 + 3.0 * 0.044715 * values * values
    )


def local(cotangent, unit_pre, gate_pre, out_weight, mix_weight, mix_bias, norm_gain, norm_shift):
    seq_len = unit_pre.shape[1]
    channels = unit_pre.shape[2]
    group_dim = GW // GROUPS
    blocks = seq_len // BLK
    sp_size = lax.axis_size("sp")
    sp_at = lax.axis_index("sp")
    group = sp_at * channels // group_dim
    weight_rows = lax.all_gather(out_weight, "sp", axis=1, tiled=True)
    weight_whole = lax.all_gather(weight_rows, "dp", axis=0, tiled=True)
    units = unit_pre[0].astype(jnp.float32)
    gates = gate_pre[0].astype(jnp.float32)
    unit_act = jax.nn.gelu(units)
    gate_act = jax.nn.gelu(gates)
    moments = sum_over(
        jnp.stack([jnp.sum(gate_act, axis=-1), jnp.sum(gate_act * gate_act, axis=-1)]), "sp"
    )
    mean_val = moments[0] / GW
    var_val = moments[1] / GW - mean_val * mean_val
    rstd_val = lax.rsqrt(var_val + epsilon)
    centred = (gate_act - mean_val[:, None]) * rstd_val[:, None]
    gain_vec = norm_gain.astype(jnp.float32)
    normed = (centred * gain_vec + norm_shift.astype(jnp.float32)).astype(jnp.bfloat16)
    causal = jnp.arange(BLK)[:, None] >= jnp.arange(BLK)[None, :]
    local_weight = lax.dynamic_index_in_dim(mix_weight, group, 0, keepdims=False)
    masked = jnp.where(causal, local_weight, jnp.zeros_like(local_weight))
    local_bias = lax.dynamic_index_in_dim(mix_bias, group, 0, keepdims=False).astype(jnp.float32)
    normed_blocks = normed.reshape(blocks, BLK, channels)
    mixed = jnp.einsum("ts,nsd->ntd", masked, normed_blocks, preferred_element_type=jnp.float32)
    mixed = (mixed + local_bias[None, :, None]).reshape(seq_len, channels)
    gated = (unit_act * mixed).astype(jnp.bfloat16)
    gated_rows = lax.all_to_all(gated, "sp", split_axis=0, concat_axis=1, tiled=True)
    head_rows = jnp.dot(cotangent[0], weight_whole, preferred_element_type=jnp.float32)
    head = lax.all_to_all(
        head_rows.astype(jnp.bfloat16), "sp", split_axis=1, concat_axis=0, tiled=True
    ).astype(jnp.float32)
    weight_part = lax.dot_general(
        cotangent[0], gated_rows, (((0,), (0,)), ((), ())), preferred_element_type=jnp.float32
    ).astype(jnp.bfloat16)
    token_count = lax.axis_size("dp") * seq_len
    norm_scale = 1.0 / math.sqrt(token_count)
    mix_scale = 1.0 / math.sqrt(token_count // BLK * group_dim)
    plane_sum = lax.psum_scatter(weight_part, "dp", scatter_dimension=0, tiled=True)
    plane_parts = jnp.moveaxis(plane_sum.reshape(plane_sum.shape[0], sp_size, channels), 1, 0)
    arrived = lax.all_to_all(plane_parts, "sp", split_axis=0, concat_axis=0, tiled=True)
    out_grad = arrived.astype(jnp.float32).sum(axis=0) * norm_scale
    unit_grad = (head * mixed * gelu_slope(units)).astype(jnp.bfloat16)
    mix_grad = head * unit_act
    mix_round = mix_grad.astype(jnp.bfloat16).reshape(blocks, BLK, channels)
    mix_term = jnp.einsum(
        "ntd,nsd->ts", mix_round, normed_blocks, preferred_element_type=jnp.float32
    )
    mix_term = jnp.where(causal, mix_term, jnp.float32(0.0))
    bias_term = jnp.sum(mix_grad.reshape(blocks, BLK, channels), axis=(0, 2))
    normed_grad = jnp.einsum(
        "ts,ntd->nsd", masked, mix_round, preferred_element_type=jnp.float32
    ).reshape(seq_len, channels)
    gain_term = jnp.sum(normed_grad * centred, axis=0)
    shift_term = jnp.sum(normed_grad, axis=0)
    scaled = normed_grad * gain_vec
    back_sums = sum_over(
        jnp.stack([jnp.sum(scaled, axis=-1), jnp.sum(scaled * centred, axis=-1)]), "sp"
    )
    first_m = back_sums[0] / GW
    second_m = back_sums[1] / GW
    gate_grad = (
        rstd_val[:, None]
        * (scaled - first_m[:, None] - centred * second_m[:, None])
        * gelu_slope(gates)
    ).astype(jnp.bfloat16)
    group_hot = (jnp.arange(GROUPS) == group).astype(jnp.float32)
    own_hot = (jnp.arange(sp_size) == sp_at).astype(jnp.float32)
    packed = jnp.concatenate(
        [
            (group_hot[:, None, None] * mix_term).reshape(GROUPS * BLK, BLK),
            group_hot[:, None] * bias_term,
            own_hot[:, None] * gain_term,
            own_hot[:, None] * shift_term,
        ]
    )
    total = lax.psum(packed, ("sp", "dp"))
    top = GROUPS * BLK
    weight_total = total[:top].reshape(GROUPS, BLK, BLK)
    bias_total = total[top : top + GROUPS]
    tail = total[top + GROUPS :]
    gain_total = lax.dynamic_index_in_dim(tail, sp_at, 0, keepdims=False)
    shift_total = lax.dynamic_index_in_dim(tail, sp_size + sp_at, 0, keepdims=False)
    return (
        unit_grad[None],
        gate_grad[None],
        out_grad,
        weight_total * mix_scale,
        bias_total * mix_scale,
        gain_total * norm_scale,
        shift_total * norm_scale,
    )


def solution(mesh):
    return jax.shard_map(
        local,
        mesh=mesh,
        in_specs=(
            P("dp", "sp", None),
            P("dp", None, "sp"),
            P("dp", None, "sp"),
            P("dp", "sp"),
            P(),
            P(),
            P("sp"),
            P("sp"),
        ),
        out_specs=(
            P("dp", None, "sp"),
            P("dp", None, "sp"),
            P("dp", "sp"),
            P(),
            P(),
            P("sp"),
            P("sp"),
        ),
        check_vma=False,
    )
```

profile of v0, /device:TPU:32, one launch (start us, length us, event | category | flops | bytes accessed | tf_op | source)
XLA Modules:
  0.0 828.7 jit_solution(9951408123859522207)
XLA Ops:
  7.2 37.3 %all_gather.6 = bf16[64,2048]{1,0:T(8,128)(2,1)} all-gather(bf16[64,128]{1,0:T(8,128)(2,1)} %param.11), channel_id=1, replica_groups=mesh['sp'=16,'dp'=32] {'sp'}, dimensions={1}, use_global_device_ids=true | all-gather | bytes 278528 | tf_op jit(solution)/shard_map/all_gather | solution.py:36
  44.6 1.8 fusion.58
  47.2 8.9 %all-to-all-start.1 = ((f32[16,2,2048]{2,1,0:T(2,128)}), f32[16,2,2048]{2,1,0:T(2,128)S(1)}, u32[]{:S(2)}, u32[]{:S(2)}) async-start(f32[16,2,2048]{2,1,0:T(2,128)} %broadcast_in_dim.11), calls=%async_computation.1 | async-start | bytes 524288 | tf_op jit(solution)/shard_map/all_to_all | solution.py:17
  56.1 54.5 %all-gather.2.cloned.1.call-done = bf16[2048,2048]{1,0:T(8,128)(2,1)} async-done(((bf16[64,2048]{1,0:T(8,128)(2,1)}), bf16[2048,2048]{1,0:T(8,128)(2,1)}) %all-gather.2.cloned.1.call-update) | async-done | bytes 8388624 | tf_op jit(solution)/shard_map/all_gather | solution.py:37
  110.6 4.6 fusion.5
  116.2 12.7 %all-to-all-start = ((bf16[128,16,128]{2,0,1:T(8,128)(2,1)}), bf16[128,16,128]{2,0,1:T(8,128)(2,1)S(1)}, u32[]{:S(2)}, u32[]{:S(2)}) async-start(bf16[128,16,128]{2,0,1:T(8,128)(2,1)} %bitcast.135), calls=%async_computation | async-start | bytes 1048576 | tf_op jit(solution)/shard_map/all_to_all | solution.py:61
  129.0 29.5 %all-to-all-done = bf16[128,16,128]{2,0,1:T(8,128)(2,1)S(1)} async-done(((bf16[128,16,128]{2,0,1:T(8,128)(2,1)}), bf16[128,16,128]{2,0,1:T(8,128)(2,1)S(1)}, u32[]{:S(2)}, u32[]{:S(2)}) %all-to-all-start) | async-done | bytes 524320 | tf_op jit(solution)/shard_map/all_to_all | solution.py:61
  160.1 3.3 fusion.56
  164.2 6.1 all-to-all-start.2
  171.0 17.5 %all-to-all-done.2 = f32[16,2,2048]{2,1,0:T(2,128)S(1)} async-done(((f32[16,2,2048]{2,1,0:T(2,128)}), f32[16,2,2048]{2,1,0:T(2,128)S(1)}, u32[]{:S(2)}, u32[]{:S(2)}) %all-to-all-start.2) | async-done | bytes 262176 | tf_op jit(solution)/shard_map/all_to_all | solution.py:17
  188.7 2.8 fusion.51
  191.5 3.0 multiply_convert_fusion
  194.4 6.1 all-to-all-start.3
  200.9 2.5 fusion.6
  204.6 24.2 %all-to-all-done.3 = bf16[16,128,128]{2,1,0:T(8,128)(2,1)S(1)} async-done(((bf16[16,128,128]{2,1,0:T(8,128)(2,1)}), bf16[16,128,128]{2,1,0:T(8,128)(2,1)S(1)}, u32[]{:S(2)}, u32[]{:S(2)}) %all-to-all-start.3) | async-done | bytes 524320 | tf_op jit(solution)/shard_map/all_to_all | solution.py:59
  229.2 5.5 convert_bitcast_fusion
  234.7 12.4 %copy.42 = bf16[2048,2048]{1,0:T(8,128)(2,1)} copy(bf16[2048,2048]{0,1:T(8,128)(2,1)} %convert_bitcast_fusion) | data formatting | bytes 16777216
  247.1 423.4 %all-reduce.2.cloned.1.call-done = f32[1064,128]{1,0:T(8,128)} async-done(((f32[1064,128]{1,0:T(8,128)}), f32[1064,128]{1,0:T(8,128)}) %all-reduce.2.cloned.1.call-update) | async-done | bytes 544784 | tf_op jit(solution)/shard_map/psum | solution.py:108
  671.2 117.9 %reduce-scatter.4.cloned.1.call-done = bf16[64,2048]{1,0:T(8,128)(2,1)} async-done(((bf16[2048,2048]{1,0:T(8,128)(2,1)}), bf16[64,2048]{1,0:T(8,128)(2,1)}) %reduce-scatter.4.cloned.1.call-update) | async-done | bytes 262160
  791.3 12.7 %all-to-all-start.4 = ((bf16[16,64,128]{2,1,0:T(8,128)(2,1)}), bf16[16,64,128]{2,1,0:T(8,128)(2,1)S(1)}, u32[]{:S(2)}, u32[]{:S(2)}) async-start(bf16[16,64,128]{2,1,0:T(8,128)(2,1)} %bitcast.29), calls=%async_computation.4 | async-start | bytes 524288 | tf_op jit(solution)/shard_map/all_to_all | solution.py:72
  804.5 1.3 slice_multiply_fusion.5
  805.7 1.9 slice_multiply_fusion
  807.6 1.5 fusion.30
  809.1 12.2 %all-to-all-done.4 = bf16[16,64,128]{2,1,0:T(8,128)(2,1)S(1)} async-done(((bf16[16,64,128]{2,1,0:T(8,128)(2,1)}), bf16[16,64,128]{2,1,0:T(8,128)(2,1)S(1)}, u32[]{:S(2)}, u32[]{:S(2)}) %all-to-all-start.4) | async-done | bytes 262176 | tf_op jit(solution)/shard_map/all_to_all | solution.py:72
  (52 shorter events, 11.2 us)
Async XLA Ops:
  7.2 103.5 %copy-start = (bf16[1,128,2048]{2,1,0:T(8,128)(2,1)S(1)}, bf16[1,128,2048]{2,1,0:T(8,128)(2,1)}, u32[]{:S(2)}) copy-start(bf16[1,128,2048]{2,1,0:T(8,128)(2,1)} %param.8) | copy-start | bytes 1572868
  7.2 103.4 %all-gather.2.cloned.1.call-start = ((), (), s32[]{:S(2)}) async-start(), calls=%async_computation.6 | async-start | bytes 8650752 | tf_op jit(solution)/shard_map/all_gather | solution.py:37
  47.2 69.0 %all-to-all-start.1 = ((f32[16,2,2048]{2,1,0:T(2,128)}), f32[16,2,2048]{2,1,0:T(2,128)S(1)}, u32[]{:S(2)}, u32[]{:S(2)}) async-start(f32[16,2,2048]{2,1,0:T(2,128)} %broadcast_in_dim.11), calls=%async_computation.1 | async-start | bytes 524288 | tf_op jit(solution)/shard_map/all_to_all | solution.py:17
  56.1 72.8 %copy-start.5 = (bf16[128]{0:T(256)(128)(2,1)S(1)}, bf16[128]{0:T(256)(128)(2,1)}, u32[]{:S(2)}) copy-start(bf16[128]{0:T(256)(128)(2,1)} %param.14) | copy-start | bytes 772
  56.1 102.5 %copy-start.2 = (bf16[1,2048,128]{2,1,0:T(8,128)(2,1)S(1)}, bf16[1,2048,128]{2,1,0:T(8,128)(2,1)}, u32[]{:S(2)}) copy-start(bf16[1,2048,128]{2,1,0:T(8,128)(2,1)} %param.9) | copy-start | bytes 1572868
  56.1 104.0 %copy-start.1 = (bf16[1,2048,128]{2,1,0:T(8,128)(2,1)S(1)}, bf16[1,2048,128]{2,1,0:T(8,128)(2,1)}, u32[]{:S(2)}) copy-start(bf16[1,2048,128]{2,1,0:T(8,128)(2,1)} %param.10) | copy-start | bytes 1572868
  115.3 55.1 %copy-start.6 = (bf16[128]{0:T(256)(128)(2,1)S(1)}, bf16[128]{0:T(256)(128)(2,1)}, u32[]{:S(2)}) copy-start(bf16[128]{0:T(256)(128)(2,1)} %param.15) | copy-start | bytes 772
  116.2 42.4 %all-to-all-start = ((bf16[128,16,128]{2,0,1:T(8,128)(2,1)}), bf16[128,16,128]{2,0,1:T(8,128)(2,1)S(1)}, u32[]{:S(2)}, u32[]{:S(2)}) async-start(bf16[128,16,128]{2,0,1:T(8,128)(2,1)} %bitcast.135), calls=%async_computation | async-start | bytes 1048576 | tf_op jit(solution)/shard_map/all_to_all | solution.py:61
  159.1 1.0 copy-start.3
  164.2 24.4 %all-to-all-start.2 = ((f32[16,2,2048]{2,1,0:T(2,128)}), f32[16,2,2048]{2,1,0:T(2,128)S(1)}, u32[]{:S(2)}, u32[]{:S(2)}) async-start(f32[16,2,2048]{2,1,0:T(2,128)} %broadcast_in_dim.15), calls=%async_computation.2 | async-start | bytes 524288 | tf_op jit(solution)/shard_map/all_to_all | solution.py:17
  194.4 34.5 %all-to-all-start.3 = ((bf16[16,128,128]{2,1,0:T(8,128)(2,1)}), bf16[16,128,128]{2,1,0:T(8,128)(2,1)S(1)}, u32[]{:S(2)}, u32[]{:S(2)}) async-start(bf16[16,128,128]{2,1,0:T(8,128)(2,1)} %get-tuple-element.36), calls=%async_computation.3 | async-start | bytes 1048576 | tf_op jit(solution)/shard_map/all_to_all | solution.py:59
  200.5 470.0 %all-reduce.2.cloned.1.call-start = ((), (), s32[]{:S(2)}) async-start(), calls=%async_computation.7 | async-start | bytes 1089536 | tf_op jit(solution)/shard_map/psum | solution.py:108
  204.6 584.5 %reduce-scatter.4.cloned.1.call-start = ((), (), s32[]{:S(2)}) async-start(), calls=%async_computation.8 | async-start | bytes 8650752
  247.1 560.5 %copy-start.4 = (f32[16,128,128]{2,1,0:T(8,128)S(1)}, f32[16,128,128]{2,1,0:T(8,128)}, u32[]{:S(2)}) copy-start(f32[16,128,128]{2,1,0:T(8,128)} %get-tuple-element.37) | copy-start | bytes 3145732
  791.3 30.0 %all-to-all-start.4 = ((bf16[16,64,128]{2,1,0:T(8,128)(2,1)}), bf16[16,64,128]{2,1,0:T(8,128)(2,1)S(1)}, u32[]{:S(2)}, u32[]{:S(2)}) async-start(bf16[16,64,128]{2,1,0:T(8,128)(2,1)} %bitcast.29), calls=%async_computation.4 | async-start | bytes 524288 | tf_op jit(solution)/shard_map/all_to_all | solution.py:72
Sparse Core Ops, SparseCore 0:
  44.7 65.8 all-gather.1
  206.8 463.6 all-reduce.1
  675.1 114.0 reduce-scatter.3
where the time goes:
time: 830 us; the launch traced here: 829 us
  waiting for transfers between devices  679 us (82%)
  starting transfers between devices  46.6 us (6%)
  blocking collectives  37.3 us (4%)
  local copies, waits for them, and re-layouts  19.8 us (2%)
  matrix products  18.9 us (2%)
  between operations  13.9 us (2%)
  other arithmetic  12.7 us (2%)
    psum x1, waiting for transfers between devices, local(): total = lax.psum(packed, ('sp', 'dp'))  423 us
    unnamed x4, waiting for transfers between devices  118 us
    all_gather x1, waiting for transfers between devices, local(): weight_whole = lax.all_gather(weight_rows, 'dp', axis=0, tiled=True)  54.5 us
    all_gather x1, blocking collectives, local(): weight_rows = lax.all_gather(out_weight, 'sp', axis=1, tiled=True)  37.3 us
    all_to_all x1, waiting for transfers between devices, local(): lax.all_to_all(head_rows.astype(jnp.bfloat16), 'sp', split_axis=1, concat...  29.5 us
    all_to_all x1, waiting for transfers between devices, local(): lax.all_to_all(gated, 'sp', split_axis=0, concat_axis=1, tiled=True)  24.2 us
    all_to_all x2, waiting for transfers between devices, sum_over(): return lax.all_to_all(copies, axis, 0, 0, tiled=True).sum(axis=0)  17.5 us
  transfers between devices with their start and end apart: 8, of which 7 were waited for; matrix products, arithmetic and copies ran while one was open for 4% of the time, Pallas kernels for 0%

commit v1 on v0

--- a/solution.py
+++ b/solution.py
@@ -9,6 +9,9 @@
 BLK = 128
 epsilon = 1e-05
 tanh_coef = math.sqrt(2.0 / math.pi)
+proceed_frames = lambda shard_in, axis_tag: jnp.concatenate(
+    lax.all_to_all(jnp.stack([shard_in] * lax.psum(1, axis_tag)), axis_tag, 0, 0), axis=0
+)
 
 
 def sum_over(x, axis):
@@ -34,7 +37,7 @@
     sp_at = lax.axis_index("sp")
     group = sp_at * channels // group_dim
     weight_rows = lax.all_gather(out_weight, "sp", axis=1, tiled=True)
-    weight_whole = lax.all_gather(weight_rows, "dp", axis=0, tiled=True)
+    weight_whole = proceed_frames(weight_rows, "dp")
     units = unit_pre[0].astype(jnp.float32)
     gates = gate_pre[0].astype(jnp.float32)
     unit_act = jax.nn.gelu(units)

time: 830 us -> 774 us (0.933)
  the two profiles are of different devices: /device:TPU:32 before, /device:TPU:1 now
where the time goes in v1:
time: 774 us; the launch traced here: 773 us
  waiting for transfers between devices  611 us (79%)
  starting transfers between devices  60.3 us (8%)
  blocking collectives  30.8 us (4%)
  local copies, waits for them, and re-layouts  24.1 us (3%)
  matrix products  19 us (2%)
  between operations  15.7 us (2%)
  other arithmetic  11.7 us (2%)
    psum x1, waiting for transfers between devices, local(): total = lax.psum(packed, ('sp', 'dp'))  442 us
    all_to_all x1, waiting for transfers between devices, lax.all_to_all(jnp.stack([shard_in] * lax.psum(1, axis_tag)), axis_tag, 0...  99.9 us
    all_gather x1, blocking collectives, local(): weight_rows = lax.all_gather(out_weight, 'sp', axis=1, tiled=True)  30.8 us
    all_to_all x2, starting transfers between devices, sum_over(): return lax.all_to_all(copies, axis, 0, 0, tiled=True).sum(axis=0)  20 us
    all_to_all x2, waiting for transfers between devices, sum_over(): return lax.all_to_all(copies, axis, 0, 0, tiled=True).sum(axis=0)  19 us
    all_to_all x1, waiting for transfers between devices, local(): lax.all_to_all(head_rows.astype(jnp.bfloat16), 'sp', split_axis=1, concat...  18.7 us
    all_to_all x1, waiting for transfers between devices, local(): lax.all_to_all(gated, 'sp', split_axis=0, concat_axis=1, tiled=True)  18.1 us
  transfers between devices with their start and end apart: 8, of which 7 were waited for; matrix products, arithmetic and copies ran while one was open for 5% of the time, Pallas kernels for 0%

profile of v1, /device:TPU:1, one launch (start us, length us, event | category | flops | bytes accessed | tf_op | source)
XLA Modules:
  0.0 772.6 jit_solution(18408277422260110638)
XLA Ops:
  8.0 30.8 %all_gather.3 = bf16[64,2048]{1,0:T(8,128)(2,1)S(1)} all-gather(bf16[64,128]{1,0:T(8,128)(2,1)} %param.11), channel_id=1, replica_groups=mesh['sp'=16,'dp'=32] {'sp'}, dimensions={1}, use_global_device_ids=true | all-gather | bytes 278528 | tf_op jit(solution)/shard_map/all_gather | solution.py:39
  38.8 4.3 stack.14
  43.1 15.1 %all-to-all-start = ((bf16[32,64,2048]{2,1,0:T(8,128)(2,1)}), bf16[32,64,2048]{2,1,0:T(8,128)(2,1)}, u32[]{:S(2)}, u32[]{:S(2)}) async-start(bf16[32,64,2048]{2,1,0:T(8,128)(2,1)} %stack.14), calls=%async_computation | async-start | bytes 16777216 | tf_op jit(solution)/shard_map/all_to_all | solution.py:13
  59.0 99.9 %all-to-all-done = bf16[32,64,2048]{2,1,0:T(8,128)(2,1)} async-done(((bf16[32,64,2048]{2,1,0:T(8,128)(2,1)}), bf16[32,64,2048]{2,1,0:T(8,128)(2,1)}, u32[]{:S(2)}, u32[]{:S(2)}) %all-to-all-start) | async-done | bytes 8388640 | tf_op jit(solution)/shard_map/all_to_all | solution.py:13
  159.7 6.5 all-to-all-start.2
  166.2 4.7 fusion.5
  171.9 7.0 all-to-all-done.2
  178.9 6.1 all-to-all-start.1
  185.2 18.7 %all-to-all-done.1 = bf16[128,16,128]{2,0,1:T(8,128)(2,1)S(1)} async-done(((bf16[128,16,128]{2,0,1:T(8,128)(2,1)}), bf16[128,16,128]{2,0,1:T(8,128)(2,1)S(1)}, u32[]{:S(2)}, u32[]{:S(2)}) %all-to-all-start.1) | async-done | bytes 524320 | tf_op jit(solution)/shard_map/all_to_all | solution.py:64
  205.4 3.3 fusion.56
  209.5 13.5 %all-to-all-start.3 = ((f32[16,2,2048]{2,1,0:T(2,128)}), f32[16,2,2048]{2,1,0:T(2,128)S(1)}, u32[]{:S(2)}, u32[]{:S(2)}) async-start(f32[16,2,2048]{2,1,0:T(2,128)} %broadcast_in_dim.15), calls=%async_computation.3 | async-start | bytes 524288 | tf_op jit(solution)/shard_map/all_to_all | solution.py:20
  223.8 12.0 %all-to-all-done.3 = f32[16,2,2048]{2,1,0:T(2,128)S(1)} async-done(((f32[16,2,2048]{2,1,0:T(2,128)}), f32[16,2,2048]{2,1,0:T(2,128)S(1)}, u32[]{:S(2)}, u32[]{:S(2)}) %all-to-all-start.3) | async-done | bytes 262176 | tf_op jit(solution)/shard_map/all_to_all | solution.py:20
  235.9 2.8 fusion.51
  238.7 3.0 multiply_convert_fusion
  241.6 9.1 %all-to-all-start.4 = ((bf16[16,128,128]{2,1,0:T(8,128)(2,1)}), bf16[16,128,128]{2,1,0:T(8,128)(2,1)S(1)}, u32[]{:S(2)}, u32[]{:S(2)}) async-start(bf16[16,128,128]{2,1,0:T(8,128)(2,1)} %get-tuple-element.36), calls=%async_computation.4 | async-start | bytes 1048576 | tf_op jit(solution)/shard_map/all_to_all | solution.py:62
  251.1 2.5 fusion.6
  255.1 18.1 %all-to-all-done.4 = bf16[16,128,128]{2,1,0:T(8,128)(2,1)S(1)} async-done(((bf16[16,128,128]{2,1,0:T(8,128)(2,1)}), bf16[16,128,128]{2,1,0:T(8,128)(2,1)S(1)}, u32[]{:S(2)}, u32[]{:S(2)}) %all-to-all-start.4) | async-done | bytes 524320 | tf_op jit(solution)/shard_map/all_to_all | solution.py:62
  273.5 5.5 convert_bitcast_fusion
  279.0 12.3 %copy.42 = bf16[2048,2048]{1,0:T(8,128)(2,1)} copy(bf16[2048,2048]{0,1:T(8,128)(2,1)} %convert_bitcast_fusion) | data formatting | bytes 16777216
  291.4 442.4 %all-reduce.2.cloned.1.call-done = f32[1064,128]{1,0:T(8,128)} async-done(((f32[1064,128]{1,0:T(8,128)}), f32[1064,128]{1,0:T(8,128)}) %all-reduce.2.cloned.1.call-update) | async-done | bytes 544784 | tf_op jit(solution)/shard_map/psum | solution.py:111
  736.6 9.8 %all-to-all-start.5 = ((bf16[16,64,128]{2,1,0:T(8,128)(2,1)}), bf16[16,64,128]{2,1,0:T(8,128)(2,1)S(1)}, u32[]{:S(2)}, u32[]{:S(2)}) async-start(bf16[16,64,128]{2,1,0:T(8,128)(2,1)} %bitcast.30), calls=%async_computation.5 | async-start | bytes 524288 | tf_op jit(solution)/shard_map/all_to_all | solution.py:75
  748.2 1.9 slice_multiply_fusion
  750.1 1.5 fusion.30
  751.6 12.7 %all-to-all-done.5 = bf16[16,64,128]{2,1,0:T(8,128)(2,1)S(1)} async-done(((bf16[16,64,128]{2,1,0:T(8,128)(2,1)}), bf16[16,64,128]{2,1,0:T(8,128)(2,1)S(1)}, u32[]{:S(2)}, u32[]{:S(2)}) %all-to-all-start.5) | async-done | bytes 262176 | tf_op jit(solution)/shard_map/all_to_all | solution.py:75
  (52 shorter events, 13.3 us)
Async XLA Ops:
  8.0 158.2 %copy-start = (bf16[1,128,2048]{2,1,0:T(8,128)(2,1)S(1)}, bf16[1,128,2048]{2,1,0:T(8,128)(2,1)}, u32[]{:S(2)}) copy-start(bf16[1,128,2048]{2,1,0:T(8,128)(2,1)} %param.8) | copy-start | bytes 1572868
  43.1 15.1 %copy-start.1 = (bf16[1,2048,128]{2,1,0:T(8,128)(2,1)S(1)}, bf16[1,2048,128]{2,1,0:T(8,128)(2,1)}, u32[]{:S(2)}) copy-start(bf16[1,2048,128]{2,1,0:T(8,128)(2,1)} %param.10) | copy-start | bytes 1572868
  43.1 115.8 %all-to-all-start = ((bf16[32,64,2048]{2,1,0:T(8,128)(2,1)}), bf16[32,64,2048]{2,1,0:T(8,128)(2,1)}, u32[]{:S(2)}, u32[]{:S(2)}) async-start(bf16[32,64,2048]{2,1,0:T(8,128)(2,1)} %stack.14), calls=%async_computation | async-start | bytes 16777216 | tf_op jit(solution)/shard_map/all_to_all | solution.py:13
  159.7 19.2 %all-to-all-start.2 = ((f32[16,2,2048]{2,1,0:T(2,128)}), f32[16,2,2048]{2,1,0:T(2,128)S(1)}, u32[]{:S(2)}, u32[]{:S(2)}) async-start(f32[16,2,2048]{2,1,0:T(2,128)} %broadcast_in_dim.11), calls=%async_computation.2 | async-start | bytes 524288 | tf_op jit(solution)/shard_map/all_to_all | solution.py:20
  166.2 18.8 %copy-start.5 = (bf16[128]{0:T(256)(128)(2,1)S(1)}, bf16[128]{0:T(256)(128)(2,1)}, u32[]{:S(2)}) copy-start(bf16[128]{0:T(256)(128)(2,1)} %param.14) | copy-start | bytes 772
  166.2 37.6 %copy-start.2 = (bf16[1,2048,128]{2,1,0:T(8,128)(2,1)S(1)}, bf16[1,2048,128]{2,1,0:T(8,128)(2,1)}, u32[]{:S(2)}) copy-start(bf16[1,2048,128]{2,1,0:T(8,128)(2,1)} %param.9) | copy-start | bytes 1572868
  171.0 52.1 %copy-start.6 = (bf16[128]{0:T(256)(128)(2,1)S(1)}, bf16[128]{0:T(256)(128)(2,1)}, u32[]{:S(2)}) copy-start(bf16[128]{0:T(256)(128)(2,1)} %param.15) | copy-start | bytes 772
  178.9 24.9 %all-to-all-start.1 = ((bf16[128,16,128]{2,0,1:T(8,128)(2,1)}), bf16[128,16,128]{2,0,1:T(8,128)(2,1)S(1)}, u32[]{:S(2)}, u32[]{:S(2)}) async-start(bf16[128,16,128]{2,0,1:T(8,128)(2,1)} %bitcast.136), calls=%async_computation.1 | async-start | bytes 1048576 | tf_op jit(solution)/shard_map/all_to_all | solution.py:64
  204.4 1.0 copy-start.3
  209.5 26.3 %all-to-all-start.3 = ((f32[16,2,2048]{2,1,0:T(2,128)}), f32[16,2,2048]{2,1,0:T(2,128)S(1)}, u32[]{:S(2)}, u32[]{:S(2)}) async-start(f32[16,2,2048]{2,1,0:T(2,128)} %broadcast_in_dim.15), calls=%async_computation.3 | async-start | bytes 524288 | tf_op jit(solution)/shard_map/all_to_all | solution.py:20
  241.6 31.6 %all-to-all-start.4 = ((bf16[16,128,128]{2,1,0:T(8,128)(2,1)}), bf16[16,128,128]{2,1,0:T(8,128)(2,1)S(1)}, u32[]{:S(2)}, u32[]{:S(2)}) async-start(bf16[16,128,128]{2,1,0:T(8,128)(2,1)} %get-tuple-element.36), calls=%async_computation.4 | async-start | bytes 1048576 | tf_op jit(solution)/shard_map/all_to_all | solution.py:62
  250.7 483.1 %all-reduce.2.cloned.1.call-start = ((), (), s32[]{:S(2)}) async-start(), calls=%async_computation.7 | async-start | bytes 1089536 | tf_op jit(solution)/shard_map/psum | solution.py:111
  254.8 479.7 %reduce-scatter.4.cloned.1.call-start = ((), (), s32[]{:S(2)}) async-start(), calls=%async_computation.8 | async-start | bytes 8650752
  291.3 458.8 %copy-start.4 = (f32[16,128,128]{2,1,0:T(8,128)S(1)}, f32[16,128,128]{2,1,0:T(8,128)}, u32[]{:S(2)}) copy-start(f32[16,128,128]{2,1,0:T(8,128)} %get-tuple-element.37) | copy-start | bytes 3145732
  736.6 27.6 %all-to-all-start.5 = ((bf16[16,64,128]{2,1,0:T(8,128)(2,1)}), bf16[16,64,128]{2,1,0:T(8,128)(2,1)S(1)}, u32[]{:S(2)}, u32[]{:S(2)}) async-start(bf16[16,64,128]{2,1,0:T(8,128)(2,1)} %bitcast.30), calls=%async_computation.5 | async-start | bytes 524288 | tf_op jit(solution)/shard_map/all_to_all | solution.py:75
Sparse Core Ops, SparseCore 0:
  257.0 476.7 all-reduce.1
Sparse Core Ops, SparseCore 1:
  291.4 125.9 reduce-scatter.3
